TPU v7x, 32 devices: a whole 2x2x4 slice. The times are simulated.
32 devices in a mesh: fs: 16 (over z, y, x), tp: 2 (over core).
Axes of the slice: x: 2, y: 2, z: 4, core: 2. Of those that a mesh axis runs over, the one named last changes fastest.
Arguments:
- residual_in: bfloat16 [4096, 2048], P(('fs', 'tp')), may hold values from -6 to 6
- gain_first: float32 [2048], replicated, may hold values from 0.1 to 1.9
- gain_mixer: float32 [2048], replicated, may hold values from 0.1 to 1.9
- gain_second: float32 [2048], replicated, may hold values from 0.1 to 1.9
- gate_weight: float32 [2048, 6144], P('fs', 'tp'), may hold values from -0.125 to 0.125
- gate_scale: float32 [6144], P('tp'), may hold values from 0.3 to 3
- up_weight: float32 [2048, 6144], P('fs', 'tp'), may hold values from -0.125 to 0.125
- up_scale: float32 [6144], P('tp'), may hold values from 0.3 to 3
- down_weight: float32 [6144, 2048], P('tp', 'fs'), may hold values from -0.078125 to 0.078125
- down_scale: float32 [2048], P('fs'), may hold values from 0.3 to 3
- query_weight: float32 [2048, 2048], P('fs', 'tp'), may hold values from -0.125 to 0.125
- query_scale: float32 [2048], P('tp'), may hold values from 0.3 to 3
- key_weight: float32 [2048, 2048], P('fs', 'tp'), may hold values from -0.125 to 0.125
- key_scale: float32 [2048], P('tp'), may hold values from 0.3 to 3
- value_weight: float32 [2048, 2048], P('fs', 'tp'), may hold values from -0.125 to 0.125
- value_scale: float32 [2048], P('tp'), may hold values from 0.3 to 3
- output_weight: float32 [2048, 2048], P('tp', 'fs'), may hold values from -0.125 to 0.125
- output_scale: float32 [2048], P('fs'), may hold values from 0.3 to 3
Outputs:
- residual_out: bfloat16 [4096, 2048], P(('fs', 'tp'))
All inputs are finite; a program needn't handle non-finite values.
Results may differ from a plain program's by a relative error of at most 0.028.
Values may be sent and summed in bfloat16 or wider, within the bound.
A program may use at most 128 MiB of HBM per device.

v0:
```python
import jax
import jax.numpy as jnp
from jax import lax
from jax.sharding import PartitionSpec as P

HEADS = 8
HEAD_DIM = 256
BLOCK = 64
EPSILON = 1e-06
HEAD_FLOOR = 0.25
ROTARY_BASE = 10000.0
HIGHEST = lax.Precision.HIGHEST


def normalize(sequence_rows, gain_vector):
    values = sequence_rows.astype(jnp.float32)
    scaled = values * lax.rsqrt(jnp.mean(values * values, axis=-1, keepdims=True) + EPSILON)
    return (scaled * gain_vector).astype(jnp.bfloat16)


def collect_rows(sequence_rows, gain_vector):
    return lax.all_gather(normalize(sequence_rows, gain_vector), "tp", axis=0, tiled=True)


def return_rows(inputs, weight, factor):
    term = jnp.dot(inputs, weight, preferred_element_type=jnp.float32) * factor
    return lax.psum_scatter(
        lax.optimization_barrier(term.astype(jnp.bfloat16))
        .astype(jnp.float32)
        .astype(jnp.bfloat16),
        "tp",
        scatter_dimension=0,
        tiled=True,
    ).astype(jnp.float32)


def head_rates(first_head, head_count, length):
    head_number = (first_head + jnp.arange(head_count)).astype(jnp.float32)
    return jnp.exp(jnp.log(1.0 / 16.0) + head_number / (HEADS - 1) * jnp.log(4.0 / length))


def rotate(values, positions):
    half_width = values.shape[-1] // 2
    frequency = ROTARY_BASE ** (-jnp.arange(half_width, dtype=jnp.float32) * 2.0 / values.shape[-1])
    angles = positions[:, None] * frequency[None, :]
    cosine = jnp.cos(angles)[:, None, :]
    sine_value = jnp.sin(angles)[:, None, :]
    front_half = values[..., :half_width]
    back_half = values[..., half_width:]
    return jnp.concatenate(
        [
            front_half * cosine - back_half * sine_value,
            back_half * cosine + front_half * sine_value,
        ],
        axis=-1,
    )


def retention(query_pre, key_pre, value_pre, decay_rates):
    length, head_count, head_width = query_pre.shape
    positions = jnp.arange(length, dtype=jnp.float32)
    query_rot = rotate(query_pre, positions).astype(jnp.bfloat16)
    key_rot = rotate(key_pre, positions).astype(jnp.bfloat16)
    value_low = value_pre.astype(jnp.bfloat16)
    blocks = length // BLOCK
    inside = jnp.arange(BLOCK, dtype=jnp.float32)
    distance = inside[:, None] - inside[None, :]
    within = jnp.where(
        distance >= 0, jnp.exp(-decay_rates[:, None, None] * jnp.maximum(distance, 0.0)), 0.0
    ) * head_width ** (-0.5)
    query_blocks = query_rot.reshape(blocks, BLOCK, head_count, head_width)
    key_blocks = key_rot.reshape(blocks, BLOCK, head_count, head_width)
    value_blocks = value_low.reshape(blocks, BLOCK, head_count, head_width)
    scores = jnp.einsum(
        "nihe,njhe->nhij", query_blocks, key_blocks, preferred_element_type=jnp.float32
    )
    weights = (scores * within[None]).astype(jnp.bfloat16)
    inner_part = jnp.einsum(
        "nhij,njhe->nihe", weights, value_blocks, preferred_element_type=jnp.float32
    )
    fading = jnp.exp(-decay_rates[None, :] * (BLOCK - 1.0 - inside[:, None])) * head_width ** (-0.5)
    key_faded = key_blocks.astype(jnp.float32) * fading[None, :, :, None]
    updates = jnp.einsum(
        "njhd,njhe->nhde", key_faded, value_blocks.astype(jnp.float32), precision=HIGHEST
    )
    block_decay = jnp.exp(-decay_rates * BLOCK)

    def advance(memory_state, update):
        return (memory_state * block_decay[:, None, None] + update, memory_state)

    _, before = lax.scan(
        advance, jnp.zeros((head_count, head_width, head_width), jnp.float32), updates
    )
    rising = jnp.exp(-decay_rates[None, :] * (inside[:, None] + 1.0))
    queried = query_blocks.astype(jnp.float32) * rising[None, :, :, None]
    carried_part = jnp.einsum("nihd,nhde->nihe", queried, before, precision=HIGHEST)
    combined = (inner_part + carried_part).reshape(length, head_count, head_width)
    normed = combined * lax.rsqrt(
        jnp.maximum(jnp.mean(combined * combined, axis=-1, keepdims=True), HEAD_FLOOR)
    )
    return normed.astype(jnp.bfloat16).reshape(length, head_count * head_width)


def body(
    residual_in,
    gain_first,
    gain_mixer,
    gain_second,
    gate_weight,
    gate_scale,
    up_weight,
    up_scale,
    down_weight,
    down_scale,
    query_weight,
    query_scale,
    key_weight,
    key_scale,
    value_weight,
    value_scale,
    output_weight,
    output_scale,
):
    gate_part = gate_weight.astype(jnp.bfloat16)
    up_part = up_weight.astype(jnp.bfloat16)
    down_factor, output_factor = (
        lax.all_gather(down_scale, "fs", axis=0, tiled=True),
        lax.all_gather(output_scale, "fs", axis=0, tiled=True),
    )
    first_input = collect_rows(residual_in, gain_first)
    gate_full, up_full = (
        lax.all_gather(gate_part, "fs", axis=0, tiled=True),
        lax.all_gather(up_part, "fs", axis=0, tiled=True),
    )
    gate_pre = jnp.dot(first_input, gate_full, preferred_element_type=jnp.float32)
    up_pre = jnp.dot(first_input, up_full, preferred_element_type=jnp.float32)
    down_full = lax.all_gather(down_weight.astype(jnp.bfloat16), "fs", axis=1, tiled=True)
    hidden_first = (jax.nn.silu(gate_pre * gate_scale) * (up_pre * up_scale)).astype(jnp.bfloat16)
    mlp_first = return_rows(hidden_first, down_full, down_factor)
    middle = (residual_in.astype(jnp.float32) + 0.5 * mlp_first).astype(jnp.bfloat16)
    mixer_input = collect_rows(middle, gain_mixer)
    local_width = query_weight.shape[1]
    projections = (
        query_weight.astype(jnp.bfloat16),
        key_weight.astype(jnp.bfloat16),
        value_weight.astype(jnp.bfloat16),
    )
    pieces = (
        lax.all_gather(projections[0], "fs", axis=0, tiled=True),
        lax.all_gather(projections[1], "fs", axis=0, tiled=True),
        lax.all_gather(projections[2], "fs", axis=0, tiled=True),
    )
    query_pre, key_pre, value_pre = tuple(
        (
            jnp.dot(mixer_input, pieces[member], preferred_element_type=jnp.float32)
            for member in range(3)
        )
    )
    output_full = lax.all_gather(output_weight.astype(jnp.bfloat16), "fs", axis=1, tiled=True)
    length = mixer_input.shape[0]
    heads_local = local_width // HEAD_DIM
    decay_rates = head_rates(lax.axis_index("tp") * heads_local, heads_local, length)
    mixed = retention(
        (query_pre * query_scale).reshape(length, heads_local, HEAD_DIM),
        (key_pre * key_scale).reshape(length, heads_local, HEAD_DIM),
        (value_pre * value_scale).reshape(length, heads_local, HEAD_DIM),
        decay_rates,
    )
    mixer_out = return_rows(mixed, output_full, output_factor)
    second = (middle.astype(jnp.float32) + mixer_out).astype(jnp.bfloat16)
    last_input = collect_rows(second, gain_second)
    gate_last = jnp.dot(last_input, gate_full, preferred_element_type=jnp.float32) * gate_scale
    up_last = jnp.dot(last_input, up_full, preferred_element_type=jnp.float32) * up_scale
    hidden_second = (jax.nn.silu(gate_last) * up_last).astype(jnp.bfloat16)
    mlp_second = return_rows(hidden_second, down_full, down_factor)
    return (second.astype(jnp.float32) + 0.5 * mlp_second).astype(jnp.bfloat16)


def solution(mesh):
    in_specs = (
        P(("fs", "tp"), None),
        P(),
        P(),
        P(),
        P("fs", "tp"),
        P("tp"),
        P("fs", "tp"),
        P("tp"),
        P("tp", "fs"),
        P("fs"),
        P("fs", "tp"),
        P("tp"),
        P("fs", "tp"),
        P("tp"),
        P("fs", "tp"),
        P("tp"),
        P("tp", "fs"),
        P("fs"),
    )
    out_specs = P(("fs", "tp"), None)
    return jax.shard_map(body, mesh=mesh, in_specs=in_specs, out_specs=out_specs, check_vma=False)
```

profile of v0, /device:TPU:0, one launch (start us, length us, event | category | flops | bytes accessed | tf_op | source)
XLA Modules:
  0.0 955.4 jit_solution(6325975038016141110)
XLA Ops:
  6.5 1.3 fusion.12
  7.9 2.0 fusion.14
  10.0 2.4 convert_element_type.119
  12.5 1.0 convert_element_type.120
  13.5 0.0 all-gather.19.cloned.1.call-start
  13.6 2.4 convert_element_type.122
  16.0 43.0 %all-gather = f32[16,1,128]{2,1,0:T(1,128)S(1)} all-gather(f32[1,1,128]{2,1,0:T(1,128)S(1)} %bitcast.58), channel_id=1, replica_groups=mesh['fs'=16,'tp'=2] {'fs'}, dimensions={0}, use_global_device_ids=true | all-gather | bytes 8704 | tf_op jit(solution)/shard_map/all_gather | solution.py:127
  59.0 118.3 %all-gather.15.cloned.1.call-done = bf16[2048,3072]{1,0:T(8,128)(2,1)} async-done(((bf16[128,3072]{1,0:T(8,128)(2,1)}), bf16[2048,3072]{1,0:T(8,128)(2,1)}) %all-gather.15.cloned.1.call-update) | async-done | bytes 12582928 | tf_op jit(solution)/shard_map/all_gather | solution.py:132
  177.3 9.9 %convolution_multiply_fusion.3 = f32[256,3072]{1,0:T(8,128)} fusion(bf16[256,2048]{1,0:T(8,128)(2,1)} %all-gather.13.cloned.1.call-done, bf16[2048,3072]{1,0:T(8,128)(2,1)} %all-gather.15.cloned.1.call-done, f32[3072]{0:T(1024)S(1)} %copy-done.20), kind=kOutput, calls=%fused_computation.7 | convolution fusion | flops 3222011904 | bytes 16789504 | tf_op jit(solution)/shard_map/dot_general | solution.py:135
  187.2 142.5 %all-gather.17.cloned.1.call-done = bf16[2048,3072]{1,0:T(8,128)(2,1)} async-done(((bf16[128,3072]{1,0:T(8,128)(2,1)}), bf16[2048,3072]{1,0:T(8,128)(2,1)}) %all-gather.17.cloned.1.call-update) | async-done | bytes 12582928 | tf_op jit(solution)/shard_map/all_gather | solution.py:133
  329.7 196.2 %all-gather.19.cloned.1.call-done = bf16[3072,2048]{1,0:T(8,128)(2,1)} async-done(((bf16[3072,128]{1,0:T(8,128)(2,1)}), bf16[3072,2048]{1,0:T(8,128)(2,1)}) %all-gather.19.cloned.1.call-update) | async-done | bytes 12582928 | tf_op jit(solution)/shard_map/all_gather | solution.py:137
  525.9 17.1 %fusion.6 = bf16[256,2048]{1,0:T(8,128)(2,1)} fusion(bf16[3072,2048]{1,0:T(8,128)(2,1)} %all-gather.19.cloned.1.call-done, f32[2048]{0:T(1024)S(1)} %bitcast.56, bf16[256,2048]{1,0:T(8,128)(2,1)S(1)} %copy-done.18, bf16[2048,3072]{1,0:T(8,128)(2,1)} %all-gather.17.cloned.1.call-done, f32[256,3072]{1,0:T(8,128)} %convolution_multiply_fusion.3, ...), kind=kOutput, calls=%fused_computation.15 | convolution fusion | flops 6449004544 | bytes 30429184 | tf_op jit(solution)/shard_map/dot_general | solution.py:26
  543.2 0.7 convert_element_type.131
  543.9 0.0 all-gather.21.cloned.1.call-start
  544.0 5.9 reduce-scatter.4.cloned.1.call-done
  549.8 1.3 fusion.16
  551.2 1.0 fusion.18
  552.3 0.8 convert_element_type.132
  553.1 0.7 convert_element_type.128
  553.9 0.7 convert_element_type.138
  554.8 41.1 %all-gather.1 = f32[16,1,128]{2,1,0:T(1,128)S(1)} all-gather(f32[1,1,128]{2,1,0:T(1,128)S(1)} %bitcast.59), channel_id=1, replica_groups=mesh['fs'=16,'tp'=2] {'fs'}, dimensions={0}, use_global_device_ids=true | all-gather | bytes 8704 | tf_op jit(solution)/shard_map/all_gather | solution.py:128
  596.0 0.1 multiply_exponential_fusion.1
  596.1 0.7 select_multiply_fusion
  596.8 1.1 fusion.42
  598.0 31.3 %all-gather.25.cloned.1.call-done = bf16[2048,1024]{1,0:T(8,128)(2,1)} async-done(((bf16[128,1024]{1,0:T(8,128)(2,1)}), bf16[2048,1024]{1,0:T(8,128)(2,1)}) %all-gather.25.cloned.1.call-update) | async-done | bytes 4194320 | tf_op jit(solution)/shard_map/all_gather | solution.py:149
  629.2 9.2 all-gather.21.cloned.1.call-done
  638.4 4.7 convolution_multiply_fusion.8
  643.2 1.7 reshape.230
  644.9 73.1 %all-gather.27.cloned.1.call-done = bf16[2048,1024]{1,0:T(8,128)(2,1)} async-done(((bf16[128,1024]{1,0:T(8,128)(2,1)}), bf16[2048,1024]{1,0:T(8,128)(2,1)}) %all-gather.27.cloned.1.call-update) | async-done | bytes 4194320 | tf_op jit(solution)/shard_map/all_gather | solution.py:150
  718.0 4.7 convolution_multiply_fusion.7
  722.7 2.7 reshape.231
  725.4 69.6 %all-gather.23.cloned.1.call-done = bf16[2048,1024]{1,0:T(8,128)(2,1)} async-done(((bf16[128,1024]{1,0:T(8,128)(2,1)}), bf16[2048,1024]{1,0:T(8,128)(2,1)}) %all-gather.23.cloned.1.call-update) | async-done | bytes 4194320 | tf_op jit(solution)/shard_map/all_gather | solution.py:151
  795.0 4.6 fusion.10
  799.5 1.4 convert_element_type.130
  801.0 1.5 fusion.48
  802.5 0.3 subtract_convert_fusion.1
  802.8 3.9 fusion.27
  806.7 10.4 %while.13 = (s32[]{:T(128)}, f32[4,256,256]{2,1,0:T(8,128)S(1)}, f32[4,4,256,256]{3,2,1,0:T(8,128)}, f32[4,4,256,256]{3,2,1,0:T(8,128)}, s32[]{:T(128)}, /*index=5*/s32[]{:T(128)}, s32[]{:T(128)}) while((s32[]{:T(128)}, f32[4,256,256]{2,1,0:T(8,128)S(1)}, f32[4,4,256,256]{3,2,1,0:T(8,128)}, f32[4,4,256,256]{3,2,1,0:T(8,128)}, ...), condition=%wide.region_4.5_spmd.clone, body=%wide.region_3.4_spmd.clone.sunk | while | flops 1048603 | bytes 5243520 | solution.py:91
  806.7 1.1 bitcast_dynamic-update-slice_fusion.2
  807.8 1.5 bitcast_add_fusion.2
  809.3 1.1 bitcast_dynamic-update-slice_fusion.2
  810.4 1.5 bitcast_add_fusion.2
  811.9 1.1 bitcast_dynamic-update-slice_fusion.2
  813.0 1.5 bitcast_add_fusion.2
  814.5 1.1 bitcast_dynamic-update-slice_fusion.2
  815.7 1.5 bitcast_add_fusion.2
  817.2 5.1 fusion.24
  822.3 1.6 multiply_reduce_fusion
  824.0 0.1 copy.52
  824.1 0.3 mul.482
  824.4 0.2 copy.59
  824.6 0.7 copy.47
  825.3 0.2 copy.58
  825.5 59.4 %all-gather.29.cloned.1.call-done = bf16[1024,2048]{1,0:T(8,128)(2,1)} async-done(((bf16[1024,128]{1,0:T(8,128)(2,1)}), bf16[1024,2048]{1,0:T(8,128)(2,1)}) %all-gather.29.cloned.1.call-update) | async-done | bytes 4194320 | tf_op jit(solution)/shard_map/all_gather | solution.py:159
  884.9 4.5 fusion.8
  889.5 6.7 reduce-scatter.6.cloned.1.call-done
  896.2 1.3 fusion.20
  897.5 2.0 fusion.22
  899.6 0.3 reduce-scatter.8.cloned.1.call-start
  899.9 10.1 %all-gather.31.cloned.1.call-done = bf16[256,2048]{1,0:T(8,128)(2,1)} async-done(((bf16[128,2048]{1,0:T(8,128)(2,1)}), bf16[256,2048]{1,0:T(8,128)(2,1)}) %all-gather.31.cloned.1.call-update) | async-done | bytes 1048592 | tf_op jit(solution)/shard_map/all_gather | solution.py:22
  909.9 10.0 %convolution_multiply_fusion.1 = f32[256,3072]{1,0:T(8,128)} fusion(bf16[256,2048]{1,0:T(8,128)(2,1)} %all-gather.31.cloned.1.call-done, bf16[2048,3072]{1,0:T(8,128)(2,1)} %all-gather.15.cloned.1.call-done, f32[3072]{0:T(1024)S(1)} %copy-done.21), kind=kOutput, calls=%fused_computation.5 | convolution fusion | flops 3222011904 | bytes 16789504 | tf_op jit(solution)/shard_map/dot_general | solution.py:172
  920.0 17.0 %fusion.7 = bf16[256,2048]{1,0:T(8,128)(2,1)} fusion(bf16[3072,2048]{1,0:T(8,128)(2,1)} %all-gather.19.cloned.1.call-done, f32[2048]{0:T(1024)S(1)} %bitcast.57, bf16[256,2048]{1,0:T(8,128)(2,1)S(1)} %copy-done.19, bf16[2048,3072]{1,0:T(8,128)(2,1)} %all-gather.17.cloned.1.call-done, f32[256,3072]{1,0:T(8,128)} %convolution_multiply_fusion.1, ...), kind=kOutput, calls=%fused_computation.16 | convolution fusion | flops 6449004544 | bytes 30429184 | tf_op jit(solution)/shard_map/dot_general | solution.py:26
  937.0 9.7 %reduce-scatter.8.cloned.1.call-done = bf16[128,2048]{1,0:T(8,128)(2,1)} async-done(((bf16[256,2048]{1,0:T(8,128)(2,1)}), bf16[128,2048]{1,0:T(8,128)(2,1)}) %reduce-scatter.8.cloned.1.call-update) | async-done | bytes 524304 | tf_op jit(solution)/shard_map/reduce_scatter | solution.py:27
  946.8 2.1 fusion.23
  (93 shorter events, 0.9 us)
Async XLA Ops:
  6.5 5.9 copy-start.2
  6.5 52.5 %all-gather.13.cloned.1.call-start = ((), (), s32[]{:S(2)}) async-start(), calls=%async_computation.3 | async-start | bytes 1572864 | tf_op jit(solution)/shard_map/all_gather | solution.py:22
  9.9 6.1 copy-start.16
  10.0 167.3 %copy-start.20 = (f32[3072]{0:T(1024)S(1)}, f32[3072]{0:T(1024)}, u32[]{:S(2)}) copy-start(f32[3072]{0:T(1024)} %param.25) | copy-start | bytes 36868
  10.0 167.3 %all-gather.15.cloned.1.call-start = ((), (), s32[]{:S(2)}) async-start(), calls=%async_computation.4 | async-start | bytes 13369344 | tf_op jit(solution)/shard_map/all_gather | solution.py:132
  12.4 317.3 %all-gather.17.cloned.1.call-start = ((), (), s32[]{:S(2)}) async-start(), calls=%async_computation.5 | async-start | bytes 13369344 | tf_op jit(solution)/shard_map/all_gather | solution.py:133
  13.5 512.4 %all-gather.19.cloned.1.call-start = ((), (), s32[]{:S(2)}) async-start(), calls=%async_computation.6 | async-start | bytes 13369344 | tf_op jit(solution)/shard_map/all_gather | solution.py:137
  16.0 533.8 %reduce-scatter.4.cloned.1.call-start = ((), (), s32[]{:S(2)}) async-start(), calls=%async_computation.7 | async-start | bytes 1572864 | tf_op jit(solution)/shard_map/reduce_scatter | solution.py:27
  59.0 466.9 %copy-start.14 = (f32[16,1,128]{2,1,0:T(1,128)}, f32[16,1,128]{2,1,0:T(1,128)S(1)}, u32[]{:S(2)}) copy-start(f32[16,1,128]{2,1,0:T(1,128)S(1)} %all-gather) | copy-start | bytes 24580
  59.0 466.9 %copy-start.22 = (f32[3072]{0:T(1024)S(1)}, f32[3072]{0:T(1024)}, u32[]{:S(2)}) copy-start(f32[3072]{0:T(1024)} %param.27) | copy-start | bytes 36868
  59.0 466.9 %copy-start.18 = (bf16[256,2048]{1,0:T(8,128)(2,1)S(1)}, bf16[256,2048]{1,0:T(8,128)(2,1)}, u32[]{:S(2)}) copy-start(bf16[256,2048]{1,0:T(8,128)(2,1)} %all-gather.13.cloned.1.call-done) | copy-start | bytes 3145732
  525.9 17.2 %copy-start.6 = (f32[128,1024]{1,0:T(8,128)S(1)}, f32[128,1024]{1,0:T(8,128)}, u32[]{:S(2)}) copy-start(f32[128,1024]{1,0:T(8,128)} %param.30) | copy-start | bytes 1572868
  525.9 23.9 %copy-start = (bf16[128,2048]{1,0:T(8,128)(2,1)S(1)}, bf16[128,2048]{1,0:T(8,128)(2,1)}, u32[]{:S(2)}) copy-start(bf16[128,2048]{1,0:T(8,128)(2,1)} %param.20) | copy-start | bytes 1572868
  525.9 25.2 %copy-start.12 = (f32[2048]{0:T(1024)S(1)}, f32[2048]{0:T(1024)}, u32[]{:S(2)}) copy-start(f32[2048]{0:T(1024)} %param.22) | copy-start | bytes 24580
  543.0 9.2 copy-start.7
  543.0 10.0 %copy-start.8 = (f32[128,1024]{1,0:T(8,128)S(1)}, f32[128,1024]{1,0:T(8,128)}, u32[]{:S(2)}) copy-start(f32[128,1024]{1,0:T(8,128)} %param.34) | copy-start | bytes 1572868
  543.0 10.9 %copy-start.9 = (f32[1024,128]{1,0:T(8,128)S(1)}, f32[1024,128]{1,0:T(8,128)}, u32[]{:S(2)}) copy-start(f32[1024,128]{1,0:T(8,128)} %param.36) | copy-start | bytes 1572868
  543.0 11.7 %copy-start.17 = (f32[128]{0:T(128)S(1)}, f32[128]{0:T(128)}, u32[]{:S(2)}) copy-start(f32[128]{0:T(128)} %param.37) | copy-start | bytes 1540
  543.1 95.3 %copy-start.24 = (f32[1024]{0:T(1024)S(1)}, f32[1024]{0:T(1024)}, u32[]{:S(2)}) copy-start(f32[1024]{0:T(1024)} %param.31) | copy-start | bytes 12292
  543.1 86.1 %all-gather.25.cloned.1.call-start = ((), (), s32[]{:S(2)}) async-start(), calls=%async_computation.10 | async-start | bytes 4456448 | tf_op jit(solution)/shard_map/all_gather | solution.py:149
  543.9 94.5 %all-gather.21.cloned.1.call-start = ((), (), s32[]{:S(2)}) async-start(), calls=%async_computation.8 | async-start | bytes 1572864 | tf_op jit(solution)/shard_map/all_gather | solution.py:22
  552.2 165.8 %all-gather.27.cloned.1.call-start = ((), (), s32[]{:S(2)}) async-start(), calls=%async_computation.11 | async-start | bytes 4456448 | tf_op jit(solution)/shard_map/all_gather | solution.py:150
  553.0 242.0 %all-gather.23.cloned.1.call-start = ((), (), s32[]{:S(2)}) async-start(), calls=%async_computation.9 | async-start | bytes 4456448 | tf_op jit(solution)/shard_map/all_gather | solution.py:151
  553.9 331.1 %all-gather.29.cloned.1.call-start = ((), (), s32[]{:S(2)}) async-start(), calls=%async_computation.12 | async-start | bytes 4456448 | tf_op jit(solution)/shard_map/all_gather | solution.py:159
  554.7 341.5 %reduce-scatter.6.cloned.1.call-start = ((), (), s32[]{:S(2)}) async-start(), calls=%async_computation.13 | async-start | bytes 1572864 | tf_op jit(solution)/shard_map/reduce_scatter | solution.py:27
  598.0 120.0 %copy-start.25 = (f32[1024]{0:T(1024)S(1)}, f32[1024]{0:T(1024)}, u32[]{:S(2)}) copy-start(f32[1024]{0:T(1024)} %param.33) | copy-start | bytes 12292
  644.9 150.1 %copy-start.26 = (f32[1024]{0:T(1024)S(1)}, f32[1024]{0:T(1024)}, u32[]{:S(2)}) copy-start(f32[1024]{0:T(1024)} %param.35) | copy-start | bytes 12292
  801.0 1.5 copy-start.10
  802.8 4.0 copy-start.3
  802.8 14.4 %copy-start.4 = (bf16[256,4,128]{2,0,1:T(8,128)(2,1)}, bf16[256,4,128]{2,0,1:T(8,128)(2,1)S(1)}, u32[]{:S(2)}) copy-start(bf16[256,4,128]{2,0,1:T(8,128)(2,1)S(1)} %get-tuple-element.66) | copy-start | bytes 786436
  802.8 14.4 %copy-start.5 = (bf16[256,4,128]{2,0,1:T(8,128)(2,1)}, bf16[256,4,128]{2,0,1:T(8,128)(2,1)S(1)}, u32[]{:S(2)}) copy-start(bf16[256,4,128]{2,0,1:T(8,128)(2,1)S(1)} %get-tuple-element.67) | copy-start | bytes 786436
  817.1 5.2 copy-start.11
  884.9 12.5 %copy-start.13 = (f32[2048]{0:T(1024)S(1)}, f32[2048]{0:T(1024)}, u32[]{:S(2)}) copy-start(f32[2048]{0:T(1024)} %param.23) | copy-start | bytes 24580
  884.9 25.0 %copy-start.21 = (f32[3072]{0:T(1024)S(1)}, f32[3072]{0:T(1024)}, u32[]{:S(2)}) copy-start(f32[3072]{0:T(1024)} %param.25) | copy-start | bytes 36868
  889.4 20.5 %all-gather.31.cloned.1.call-start = ((), (), s32[]{:S(2)}) async-start(), calls=%async_computation.14 | async-start | bytes 1572864 | tf_op jit(solution)/shard_map/all_gather | solution.py:22
  899.5 20.4 %copy-start.15 = (f32[16,1,128]{2,1,0:T(1,128)S(1)}, f32[16,1,128]{2,1,0:T(1,128)}, u32[]{:S(2)}) copy-start(f32[16,1,128]{2,1,0:T(1,128)} %copy-done.14) | copy-start | bytes 24580
  899.5 20.4 %copy-start.23 = (f32[3072]{0:T(1024)S(1)}, f32[3072]{0:T(1024)}, u32[]{:S(2)}) copy-start(f32[3072]{0:T(1024)} %param.27) | copy-start | bytes 36868
  899.6 47.2 %reduce-scatter.8.cloned.1.call-start = ((), (), s32[]{:S(2)}) async-start(), calls=%async_computation.15 | async-start | bytes 1572864 | tf_op jit(solution)/shard_map/reduce_scatter | solution.py:27
  909.9 10.0 %copy-start.19 = (bf16[256,2048]{1,0:T(8,128)(2,1)S(1)}, bf16[256,2048]{1,0:T(8,128)(2,1)}, u32[]{:S(2)}) copy-start(bf16[256,2048]{1,0:T(8,128)(2,1)} %all-gather.31.cloned.1.call-done) | copy-start | bytes 3145732
  920.0 26.8 %copy-start.1 = (bf16[128,2048]{1,0:T(8,128)(2,1)S(1)}, bf16[128,2048]{1,0:T(8,128)(2,1)}, u32[]{:S(2)}) copy-start(bf16[128,2048]{1,0:T(8,128)(2,1)} %reduce-scatter.6.cloned.1.call-done) | copy-start | bytes 1572868
Sparse Core Ops, SparseCore 0:
  10.1 11.7 all-gather.12
  24.6 152.6 all-gather.14
  180.1 149.5 all-gather.16
  332.2 193.6 all-gather.18
  543.2 6.5 reduce-scatter.3
  552.4 76.7 all-gather.24
  630.8 7.6 all-gather.20
  641.2 76.7 all-gather.26
  720.8 74.1 all-gather.22
  797.5 87.3 all-gather.28
  889.6 6.5 reduce-scatter.5
  899.7 10.2 all-gather.30
  937.1 9.5 reduce-scatter.7
where the time goes:
time: 956 us; the launch traced here: 955 us
  waiting for transfers between devices  732 us (77%)
  blocking collectives  84.1 us (9%)
  matrix products  83.2 us (9%)
  other arithmetic  32.5 us (3%)
  between operations  13.6 us (1%)
    all_gather x1, waiting for transfers between devices, body(): lax.all_gather(down_weight.astype(jnp.bfloat16), 'fs', axis=1, tiled=True)  196 us
    all_gather x1, waiting for transfers between devices, body(): lax.all_gather(up_part, 'fs', axis=0, tiled=True)  142 us
    all_gather x1, waiting for transfers between devices, body(): lax.all_gather(gate_part, 'fs', axis=0, tiled=True)  118 us
    all_gather x1, waiting for transfers between devices, body(): lax.all_gather(projections[1], 'fs', axis=0, tiled=True)  73.1 us
    all_gather x1, waiting for transfers between devices, body(): lax.all_gather(projections[2], 'fs', axis=0, tiled=True)  69.6 us
    all_gather x1, waiting for transfers between devices, body(): lax.all_gather(output_weight.astype(jnp.bfloat16), 'fs', axis=1, tiled=True)  59.4 us
    all_gather x1, blocking collectives, body(): lax.all_gather(down_scale, 'fs', axis=0, tiled=True)  43 us
    all_gather x1, blocking collectives, body(): lax.all_gather(output_scale, 'fs', axis=0, tiled=True)  41.1 us
  transfers between devices with their start and end apart: 13, of which 12 were waited for; matrix products, arithmetic and copies ran while one was open for 7% of the time, Pallas kernels for 0%

commit v1 on v0

--- a/solution.py
+++ b/solution.py
@@ -134,7 +134,7 @@
     )
     gate_pre = jnp.dot(first_input, gate_full, preferred_element_type=jnp.float32)
     up_pre = jnp.dot(first_input, up_full, preferred_element_type=jnp.float32)
-    down_full = lax.all_gather(down_weight.astype(jnp.bfloat16), "fs", axis=1, tiled=True)
+    down_full = jnp.concatenate(lax.all_gather(down_weight.astype(jnp.bfloat16), "fs"), axis=1)
     hidden_first = (jax.nn.silu(gate_pre * gate_scale) * (up_pre * up_scale)).astype(jnp.bfloat16)
     mlp_first = return_rows(hidden_first, down_full, down_factor)
     middle = (residual_in.astype(jnp.float32) + 0.5 * mlp_first).astype(jnp.bfloat16)

time: 956 us -> 905 us (0.947)
  waiting for transfers between devices: 732 us -> 670 us
  local copies, waits for them, and re-layouts: 8.91 us -> 25.6 us
    all_gather x1, waiting for transfers between devices: 196 us -> 105 us  [body(): lax.all_gather(down_weight.astype(jnp.bfloat16), 'fs')]
    all_gather x1, waiting for transfers between devices: 118 us -> 148 us  [body(): lax.all_gather(gate_part, 'fs', axis=0, tiled=True)]
    reshape x0 -> x1, local copies, waits for them, and re-layouts: none -> 16.7 us  [body(): jnp.concatenate(lax.all_gather(down_weight.astype(jnp.bfloat16), 'fs'), a...]
  transfers between devices with their start and end apart: 13 -> 13, of which waited for: 12 -> 12; matrix products, arithmetic and copies ran while one was open for 7% -> 9% of each run, Pallas kernels for 0% -> 0%
where the time goes in v1:
time: 905 us; the launch traced here: 904 us
  waiting for transfers between devices  670 us (74%)
  blocking collectives  84.6 us (9%)
  matrix products  76.9 us (8%)
  other arithmetic  32.5 us (4%)
  local copies, waits for them, and re-layouts  25.6 us (3%)
  between operations  13.6 us (2%)
    all_gather x1, waiting for transfers between devices, body(): lax.all_gather(gate_part, 'fs', axis=0, tiled=True)  148 us
    all_gather x1, waiting for transfers between devices, body(): lax.all_gather(up_part, 'fs', axis=0, tiled=True)  142 us
    all_gather x1, waiting for transfers between devices, body(): lax.all_gather(down_weight.astype(jnp.bfloat16), 'fs')  105 us
    all_gather x1, waiting for transfers between devices, body(): lax.all_gather(projections[1], 'fs', axis=0, tiled=True)  73.1 us
    all_gather x1, waiting for transfers between devices, body(): lax.all_gather(projections[2], 'fs', axis=0, tiled=True)  69.6 us
    all_gather x1, waiting for transfers between devices, body(): lax.all_gather(output_weight.astype(jnp.bfloat16), 'fs', axis=1, tiled=True)  59.4 us
    all_gather x1, blocking collectives, body(): lax.all_gather(down_scale, 'fs', axis=0, tiled=True)  43.4 us
    all_gather x1, blocking collectives, body(): lax.all_gather(output_scale, 'fs', axis=0, tiled=True)  41.2 us
  transfers between devices with their start and end apart: 13, of which 12 were waited for; matrix products, arithmetic and copies ran while one was open for 9% of the time, Pallas kernels for 0%

profile of v1, /device:TPU:0, one launch (start us, length us, event | category | flops | bytes accessed | tf_op | source)
XLA Modules:
  0.0 903.9 jit_solution(16825065405966446541)
XLA Ops:
  6.5 2.5 convert_element_type.122
  9.0 0.0 all-gather.14.cloned.1.call-start
  9.1 1.2 fusion.12
  10.3 2.0 fusion.14
  12.5 1.0 convert_element_type.119
  13.5 2.4 convert_element_type.120
  15.9 0.0 reduce-scatter.4.cloned.1.call-start
  16.0 43.4 %all-gather.1 = f32[16,1,128]{2,1,0:T(1,128)S(1)} all-gather(f32[1,1,128]{2,1,0:T(1,128)S(1)} %bitcast.65), channel_id=1, replica_groups=mesh['fs'=16,'tp'=2] {'fs'}, dimensions={0}, use_global_device_ids=true | all-gather | bytes 8704 | tf_op jit(solution)/shard_map/all_gather | solution.py:127
  59.5 104.9 %all-gather.32.cloned.1.call-done = bf16[49152,128]{1,0:T(8,128)(2,1)} async-done(((bf16[3072,128]{1,0:T(8,128)(2,1)}), bf16[49152,128]{1,0:T(8,128)(2,1)}) %all-gather.32.cloned.1.call-update) | async-done | bytes 12582928 | tf_op jit(solution)/shard_map/all_gather | solution.py:137
  164.3 16.7 %copy.62 = bf16[3072,16,128]{0,2,1:T(8,128)(2,1)} copy(bf16[3072,16,128]{2,0,1:T(8,128)(2,1)} %bitcast.48) | data formatting | bytes 25165824 | tf_op jit(solution)/shard_map/reshape | solution.py:137
  181.0 147.5 %all-gather.16.cloned.1.call-done = bf16[2048,3072]{1,0:T(8,128)(2,1)} async-done(((bf16[128,3072]{1,0:T(8,128)(2,1)}), bf16[2048,3072]{1,0:T(8,128)(2,1)}) %all-gather.16.cloned.1.call-update) | async-done | bytes 12582928 | tf_op jit(solution)/shard_map/all_gather | solution.py:132
  328.5 9.9 %convolution_multiply_fusion.3 = f32[256,3072]{1,0:T(8,128)} fusion(bf16[256,2048]{1,0:T(8,128)(2,1)} %all-gather.14.cloned.1.call-done, bf16[2048,3072]{1,0:T(8,128)(2,1)} %all-gather.16.cloned.1.call-done, f32[3072]{0:T(1024)S(1)} %copy-done.20), kind=kOutput, calls=%fused_computation.7 | convolution fusion | flops 3222011904 | bytes 16789504 | tf_op jit(solution)/shard_map/dot_general | solution.py:135
  338.5 142.3 %all-gather.18.cloned.1.call-done = bf16[2048,3072]{1,0:T(8,128)(2,1)} async-done(((bf16[128,3072]{1,0:T(8,128)(2,1)}), bf16[2048,3072]{1,0:T(8,128)(2,1)}) %all-gather.18.cloned.1.call-update) | async-done | bytes 12582928 | tf_op jit(solution)/shard_map/all_gather | solution.py:133
  480.8 13.8 %fusion.6 = bf16[256,2048]{1,0:T(8,128)(2,1)} fusion(bf16[3072,2048]{0,1:T(8,128)(2,1)} %bitcast.46, f32[2048]{0:T(1024)S(1)} %bitcast.63, bf16[256,2048]{1,0:T(8,128)(2,1)S(1)} %copy-done.18, bf16[2048,3072]{1,0:T(8,128)(2,1)} %all-gather.18.cloned.1.call-done, f32[256,3072]{1,0:T(8,128)} %convolution_multiply_fusion.3, f32[3072]{0:T(1024)S(1)} %copy-done.22), kind=kOutput, calls=%fused_computation.15 | convolution fusion | flops 6449004544 | bytes 30429184 | tf_op jit(solution)/shard_map/dot_general | solution.py:26
  494.7 0.7 convert_element_type.131
  495.5 5.9 reduce-scatter.4.cloned.1.call-done
  501.4 1.3 fusion.16
  502.8 1.0 fusion.18
  503.8 0.8 convert_element_type.132
  504.7 0.7 convert_element_type.128
  505.5 0.7 convert_element_type.138
  506.4 41.2 %all-gather.2 = f32[16,1,128]{2,1,0:T(1,128)S(1)} all-gather(f32[1,1,128]{2,1,0:T(1,128)S(1)} %bitcast.66), channel_id=1, replica_groups=mesh['fs'=16,'tp'=2] {'fs'}, dimensions={0}, use_global_device_ids=true | all-gather | bytes 8704 | tf_op jit(solution)/shard_map/all_gather | solution.py:128
  547.6 0.1 multiply_exponential_fusion.1
  547.7 0.7 select_multiply_fusion
  548.4 1.1 fusion.42
  549.6 31.2 %all-gather.24.cloned.1.call-done = bf16[2048,1024]{1,0:T(8,128)(2,1)} async-done(((bf16[128,1024]{1,0:T(8,128)(2,1)}), bf16[2048,1024]{1,0:T(8,128)(2,1)}) %all-gather.24.cloned.1.call-update) | async-done | bytes 4194320 | tf_op jit(solution)/shard_map/all_gather | solution.py:149
  580.8 9.2 %all-gather.20.cloned.1.call-done = bf16[256,2048]{1,0:T(8,128)(2,1)} async-done(((bf16[128,2048]{1,0:T(8,128)(2,1)}), bf16[256,2048]{1,0:T(8,128)(2,1)}) %all-gather.20.cloned.1.call-update) | async-done | bytes 1048592 | tf_op jit(solution)/shard_map/all_gather | solution.py:22
  590.0 4.7 convolution_multiply_fusion.8
  594.7 1.7 reshape.238
  596.5 73.1 %all-gather.26.cloned.1.call-done = bf16[2048,1024]{1,0:T(8,128)(2,1)} async-done(((bf16[128,1024]{1,0:T(8,128)(2,1)}), bf16[2048,1024]{1,0:T(8,128)(2,1)}) %all-gather.26.cloned.1.call-update) | async-done | bytes 4194320 | tf_op jit(solution)/shard_map/all_gather | solution.py:150
  669.6 4.7 convolution_multiply_fusion.7
  674.3 2.7 reshape.239
  677.0 69.6 %all-gather.22.cloned.1.call-done = bf16[2048,1024]{1,0:T(8,128)(2,1)} async-done(((bf16[128,1024]{1,0:T(8,128)(2,1)}), bf16[2048,1024]{1,0:T(8,128)(2,1)}) %all-gather.22.cloned.1.call-update) | async-done | bytes 4194320 | tf_op jit(solution)/shard_map/all_gather | solution.py:151
  746.6 4.6 fusion.10
  751.1 1.4 convert_element_type.130
  752.6 1.5 fusion.48
  754.1 0.3 subtract_convert_fusion.1
  754.4 3.9 fusion.27
  758.3 10.4 %while.13 = (s32[]{:T(128)}, f32[4,256,256]{2,1,0:T(8,128)S(1)}, f32[4,4,256,256]{3,2,1,0:T(8,128)}, f32[4,4,256,256]{3,2,1,0:T(8,128)}, s32[]{:T(128)}, /*index=5*/s32[]{:T(128)}, s32[]{:T(128)}) while((s32[]{:T(128)}, f32[4,256,256]{2,1,0:T(8,128)S(1)}, f32[4,4,256,256]{3,2,1,0:T(8,128)}, f32[4,4,256,256]{3,2,1,0:T(8,128)}, ...), condition=%wide.region_4.5_spmd.clone, body=%wide.region_3.4_spmd.clone.sunk | while | flops 1048603 | bytes 5243520 | solution.py:91
  758.3 1.1 bitcast_dynamic-update-slice_fusion.2
  759.4 1.5 bitcast_add_fusion.2
  760.9 1.1 bitcast_dynamic-update-slice_fusion.2
  762.0 1.5 bitcast_add_fusion.2
  763.5 1.1 bitcast_dynamic-update-slice_fusion.2
  764.6 1.5 bitcast_add_fusion.2
  766.1 1.1 bitcast_dynamic-update-slice_fusion.2
  767.2 1.5 bitcast_add_fusion.2
  768.8 5.1 fusion.24
  773.9 1.6 multiply_reduce_fusion
  775.6 0.1 copy.78
  775.7 0.3 mul.482
  776.0 0.2 copy.85
  776.2 0.7 copy.73
  776.9 0.2 copy.84
  777.1 59.4 %all-gather.28.cloned.1.call-done = bf16[1024,2048]{1,0:T(8,128)(2,1)} async-done(((bf16[1024,128]{1,0:T(8,128)(2,1)}), bf16[1024,2048]{1,0:T(8,128)(2,1)}) %all-gather.28.cloned.1.call-update) | async-done | bytes 4194320 | tf_op jit(solution)/shard_map/all_gather | solution.py:159
  836.5 4.5 fusion.8
  841.1 6.7 reduce-scatter.6.cloned.1.call-done
  847.8 1.3 fusion.20
  849.1 2.0 fusion.22
  851.2 10.3 %all-gather.30.cloned.1.call-done = bf16[256,2048]{1,0:T(8,128)(2,1)} async-done(((bf16[128,2048]{1,0:T(8,128)(2,1)}), bf16[256,2048]{1,0:T(8,128)(2,1)}) %all-gather.30.cloned.1.call-update) | async-done | bytes 1048592 | tf_op jit(solution)/shard_map/all_gather | solution.py:22
  861.5 10.0 %convolution_multiply_fusion.1 = f32[256,3072]{1,0:T(8,128)} fusion(bf16[256,2048]{1,0:T(8,128)(2,1)} %all-gather.30.cloned.1.call-done, bf16[2048,3072]{1,0:T(8,128)(2,1)} %all-gather.16.cloned.1.call-done, f32[3072]{0:T(1024)S(1)} %copy-done.21), kind=kOutput, calls=%fused_computation.5 | convolution fusion | flops 3222011904 | bytes 16789504 | tf_op jit(solution)/shard_map/dot_general | solution.py:172
  871.6 14.0 %fusion.7 = bf16[256,2048]{1,0:T(8,128)(2,1)} fusion(bf16[3072,2048]{0,1:T(8,128)(2,1)} %bitcast.47, f32[2048]{0:T(1024)S(1)} %bitcast.64, bf16[256,2048]{1,0:T(8,128)(2,1)S(1)} %copy-done.19, bf16[2048,3072]{1,0:T(8,128)(2,1)} %all-gather.18.cloned.1.call-done, f32[256,3072]{1,0:T(8,128)} %convolution_multiply_fusion.1, f32[3072]{0:T(1024)S(1)} %copy-done.23), kind=kOutput, calls=%fused_computation.16 | convolution fusion | flops 6449004544 | bytes 30429184 | tf_op jit(solution)/shard_map/dot_general | solution.py:26
  885.5 9.7 %reduce-scatter.8.cloned.1.call-done = bf16[128,2048]{1,0:T(8,128)(2,1)} async-done(((bf16[256,2048]{1,0:T(8,128)(2,1)}), bf16[128,2048]{1,0:T(8,128)(2,1)}) %reduce-scatter.8.cloned.1.call-update) | async-done | bytes 524304 | tf_op jit(solution)/shard_map/reduce_scatter | solution.py:27
  895.2 2.1 fusion.23
  (94 shorter events, 0.9 us)
Async XLA Ops:
  6.5 5.9 copy-start.2
  6.5 157.8 %all-gather.32.cloned.1.call-start = ((), (), s32[]{:S(2)}) async-start(), calls=%async_computation.15 | async-start | bytes 13369344 | tf_op jit(solution)/shard_map/all_gather | solution.py:137
  9.0 7.0 copy-start.16
  9.0 172.0 %all-gather.14.cloned.1.call-start = ((), (), s32[]{:S(2)}) async-start(), calls=%async_computation.3 | async-start | bytes 1572864 | tf_op jit(solution)/shard_map/all_gather | solution.py:22
  12.4 316.1 %all-gather.16.cloned.1.call-start = ((), (), s32[]{:S(2)}) async-start(), calls=%async_computation.4 | async-start | bytes 13369344 | tf_op jit(solution)/shard_map/all_gather | solution.py:132
  13.5 467.3 %all-gather.18.cloned.1.call-start = ((), (), s32[]{:S(2)}) async-start(), calls=%async_computation.5 | async-start | bytes 13369344 | tf_op jit(solution)/shard_map/all_gather | solution.py:133
  15.9 485.5 %reduce-scatter.4.cloned.1.call-start = ((), (), s32[]{:S(2)}) async-start(), calls=%async_computation.6 | async-start | bytes 1572864 | tf_op jit(solution)/shard_map/reduce_scatter | solution.py:27
  59.5 421.3 %copy-start.14 = (f32[16,1,128]{2,1,0:T(1,128)}, f32[16,1,128]{2,1,0:T(1,128)S(1)}, u32[]{:S(2)}) copy-start(f32[16,1,128]{2,1,0:T(1,128)S(1)} %all-gather.1) | copy-start | bytes 24580
  164.3 164.2 %copy-start.20 = (f32[3072]{0:T(1024)S(1)}, f32[3072]{0:T(1024)}, u32[]{:S(2)}) copy-start(f32[3072]{0:T(1024)} %param.25) | copy-start | bytes 36868
  181.0 299.8 %copy-start.22 = (f32[3072]{0:T(1024)S(1)}, f32[3072]{0:T(1024)}, u32[]{:S(2)}) copy-start(f32[3072]{0:T(1024)} %param.27) | copy-start | bytes 36868
  181.0 299.8 %copy-start.18 = (bf16[256,2048]{1,0:T(8,128)(2,1)S(1)}, bf16[256,2048]{1,0:T(8,128)(2,1)}, u32[]{:S(2)}) copy-start(bf16[256,2048]{1,0:T(8,128)(2,1)} %all-gather.14.cloned.1.call-done) | copy-start | bytes 3145732
  480.8 13.9 %copy-start.6 = (f32[128,1024]{1,0:T(8,128)S(1)}, f32[128,1024]{1,0:T(8,128)}, u32[]{:S(2)}) copy-start(f32[128,1024]{1,0:T(8,128)} %param.30) | copy-start | bytes 1572868
  480.8 20.6 %copy-start = (bf16[128,2048]{1,0:T(8,128)(2,1)S(1)}, bf16[128,2048]{1,0:T(8,128)(2,1)}, u32[]{:S(2)}) copy-start(bf16[128,2048]{1,0:T(8,128)(2,1)} %param.20) | copy-start | bytes 1572868
  480.8 21.9 %copy-start.12 = (f32[2048]{0:T(1024)S(1)}, f32[2048]{0:T(1024)}, u32[]{:S(2)}) copy-start(f32[2048]{0:T(1024)} %param.22) | copy-start | bytes 24580
  494.6 9.2 %copy-start.7 = (f32[128,1024]{1,0:T(8,128)S(1)}, f32[128,1024]{1,0:T(8,128)}, u32[]{:S(2)}) copy-start(f32[128,1024]{1,0:T(8,128)} %param.32) | copy-start | bytes 1572868
  494.6 10.0 %copy-start.8 = (f32[128,1024]{1,0:T(8,128)S(1)}, f32[128,1024]{1,0:T(8,128)}, u32[]{:S(2)}) copy-start(f32[128,1024]{1,0:T(8,128)} %param.34) | copy-start | bytes 1572868
  494.6 10.9 %copy-start.9 = (f32[1024,128]{1,0:T(8,128)S(1)}, f32[1024,128]{1,0:T(8,128)}, u32[]{:S(2)}) copy-start(f32[1024,128]{1,0:T(8,128)} %param.36) | copy-start | bytes 1572868
  494.6 11.7 %copy-start.17 = (f32[128]{0:T(128)S(1)}, f32[128]{0:T(128)}, u32[]{:S(2)}) copy-start(f32[128]{0:T(128)} %param.37) | copy-start | bytes 1540
  494.7 95.4 %copy-start.24 = (f32[1024]{0:T(1024)S(1)}, f32[1024]{0:T(1024)}, u32[]{:S(2)}) copy-start(f32[1024]{0:T(1024)} %param.31) | copy-start | bytes 12292
  494.7 86.1 %all-gather.24.cloned.1.call-start = ((), (), s32[]{:S(2)}) async-start(), calls=%async_computation.9 | async-start | bytes 4456448 | tf_op jit(solution)/shard_map/all_gather | solution.py:149
  495.5 94.5 %all-gather.20.cloned.1.call-start = ((), (), s32[]{:S(2)}) async-start(), calls=%async_computation.7 | async-start | bytes 1572864 | tf_op jit(solution)/shard_map/all_gather | solution.py:22
  503.8 165.8 %all-gather.26.cloned.1.call-start = ((), (), s32[]{:S(2)}) async-start(), calls=%async_computation.10 | async-start | bytes 4456448 | tf_op jit(solution)/shard_map/all_gather | solution.py:150
  504.6 242.0 %all-gather.22.cloned.1.call-start = ((), (), s32[]{:S(2)}) async-start(), calls=%async_computation.8 | async-start | bytes 4456448 | tf_op jit(solution)/shard_map/all_gather | solution.py:151
  505.5 331.1 %all-gather.28.cloned.1.call-start = ((), (), s32[]{:S(2)}) async-start(), calls=%async_computation.11 | async-start | bytes 4456448 | tf_op jit(solution)/shard_map/all_gather | solution.py:159
  506.3 341.5 %reduce-scatter.6.cloned.1.call-start = ((), (), s32[]{:S(2)}) async-start(), calls=%async_computation.12 | async-start | bytes 1572864 | tf_op jit(solution)/shard_map/reduce_scatter | solution.py:27
  549.6 120.0 %copy-start.25 = (f32[1024]{0:T(1024)S(1)}, f32[1024]{0:T(1024)}, u32[]{:S(2)}) copy-start(f32[1024]{0:T(1024)} %param.33) | copy-start | bytes 12292
  596.4 150.1 %copy-start.26 = (f32[1024]{0:T(1024)S(1)}, f32[1024]{0:T(1024)}, u32[]{:S(2)}) copy-start(f32[1024]{0:T(1024)} %param.35) | copy-start | bytes 12292
  752.6 1.5 copy-start.10
  754.4 4.0 copy-start.3
  754.4 14.4 %copy-start.4 = (bf16[256,4,128]{2,0,1:T(8,128)(2,1)}, bf16[256,4,128]{2,0,1:T(8,128)(2,1)S(1)}, u32[]{:S(2)}) copy-start(bf16[256,4,128]{2,0,1:T(8,128)(2,1)S(1)} %get-tuple-element.66) | copy-start | bytes 786436
  754.4 14.4 %copy-start.5 = (bf16[256,4,128]{2,0,1:T(8,128)(2,1)}, bf16[256,4,128]{2,0,1:T(8,128)(2,1)S(1)}, u32[]{:S(2)}) copy-start(bf16[256,4,128]{2,0,1:T(8,128)(2,1)S(1)} %get-tuple-element.67) | copy-start | bytes 786436
  768.7 5.2 copy-start.11
  836.5 12.5 %copy-start.13 = (f32[2048]{0:T(1024)S(1)}, f32[2048]{0:T(1024)}, u32[]{:S(2)}) copy-start(f32[2048]{0:T(1024)} %param.23) | copy-start | bytes 24580
  836.5 25.0 %copy-start.21 = (f32[3072]{0:T(1024)S(1)}, f32[3072]{0:T(1024)}, u32[]{:S(2)}) copy-start(f32[3072]{0:T(1024)} %param.25) | copy-start | bytes 36868
  841.0 20.5 %all-gather.30.cloned.1.call-start = ((), (), s32[]{:S(2)}) async-start(), calls=%async_computation.13 | async-start | bytes 1572864 | tf_op jit(solution)/shard_map/all_gather | solution.py:22
  851.1 20.4 %copy-start.15 = (f32[16,1,128]{2,1,0:T(1,128)S(1)}, f32[16,1,128]{2,1,0:T(1,128)}, u32[]{:S(2)}) copy-start(f32[16,1,128]{2,1,0:T(1,128)} %copy-done.14) | copy-start | bytes 24580
  851.1 20.4 %copy-start.23 = (f32[3072]{0:T(1024)S(1)}, f32[3072]{0:T(1024)}, u32[]{:S(2)}) copy-start(f32[3072]{0:T(1024)} %param.27) | copy-start | bytes 36868
  851.1 44.1 %reduce-scatter.8.cloned.1.call-start = ((), (), s32[]{:S(2)}) async-start(), calls=%async_computation.14 | async-start | bytes 1572864 | tf_op jit(solution)/shard_map/reduce_scatter | solution.py:27
  861.5 10.0 %copy-start.19 = (bf16[256,2048]{1,0:T(8,128)(2,1)S(1)}, bf16[256,2048]{1,0:T(8,128)(2,1)}, u32[]{:S(2)}) copy-start(bf16[256,2048]{1,0:T(8,128)(2,1)} %all-gather.30.cloned.1.call-done) | copy-start | bytes 3145732
  871.5 23.7 %copy-start.1 = (bf16[128,2048]{1,0:T(8,128)(2,1)S(1)}, bf16[128,2048]{1,0:T(8,128)(2,1)}, u32[]{:S(2)}) copy-start(bf16[128,2048]{1,0:T(8,128)(2,1)} %reduce-scatter.6.cloned.1.call-done) | copy-start | bytes 1572868
Sparse Core Ops, SparseCore 0:
  10.1 154.1 all-gather.31
  165.9 7.1 all-gather.13
  175.9 152.5 all-gather.15
  331.2 149.5 all-gather.17
  494.8 6.5 reduce-scatter.3
  504.0 76.7 all-gather.23
  582.4 7.6 all-gather.19
  592.8 76.7 all-gather.25
  672.4 74.1 all-gather.21
  749.1 87.3 all-gather.27
  841.1 6.5 reduce-scatter.5
  851.2 10.2 all-gather.29
  885.7 9.5 reduce-scatter.7
